TPU v7x, 32 devices: a whole 2x2x4 slice. The times are simulated.
32 devices in a mesh: sp: 16 (over z, y, x), tp: 2 (over core).
Axes of the slice: x: 2, y: 2, z: 4, core: 2. Of those that a mesh axis runs over, the one named last changes fastest.
Arguments:
- tokens: bfloat16 [16384, 2048], P('sp', 'tp'), may hold values from -6 to 6
- norm_gain: float32 [2048], replicated, may hold values from 0.1 to 1.9
- w_conv_a: bfloat16 [2048, 1024], P('sp', 'tp'), may hold values from -0.125 to 0.125
- w_conv_gate: bfloat16 [2048, 1024], P('sp', 'tp'), may hold values from -0.125 to 0.125
- conv_weight: float32 [31, 1024], P(None, 'tp'), may hold values from -16 to 16
- conv_gain: float32 [1024], P('tp'), may hold values from 0.1 to 1.9
- w_query: bfloat16 [2048, 512], P('sp', 'tp'), may hold values from -0.125 to 0.125
- w_key: bfloat16 [2048, 512], P('sp', 'tp'), may hold values from -0.125 to 0.125
- w_value: bfloat16 [2048, 1024], P('sp', 'tp'), may hold values from -0.125 to 0.125
- w_outgate: bfloat16 [2048, 1024], P('sp', 'tp'), may hold values from -0.125 to 0.125
- w_decay: bfloat16 [2048, 512], P('sp', 'tp'), may hold values from -0.125 to 0.125
- decay_bias: float32 [512], P('tp'), may hold values from 0 to 12
- decay_extra: float32 [16384, 512], P('sp', 'tp'), may hold values from -2 to 0
- head_gain: float32 [128], replicated, may hold values from 0.1 to 1.9
- init_state: float32 [8, 64, 128], P('tp'), may hold values from -768 to 768
- w_out_conv: bfloat16 [1024, 2048], P('tp', 'sp'), may hold values from -0.125 to 0.125
- w_out_gla: bfloat16 [1024, 2048], P('tp', 'sp'), may hold values from -0.125 to 0.125
Outputs:
- mixed: bfloat16 [16384, 2048], P(('sp', 'tp'))
All inputs are finite; a program needn't handle non-finite values.
Results may differ from a plain program's by a relative error of at most 0.022.
Values may be sent and summed in bfloat16 or wider, within the bound.
A program may use at most 128 MiB of HBM per device.

v0:
```python
import jax
import jax.numpy as jnp
from jax import lax
from jax.sharding import PartitionSpec as P

D_CONV = 1024
HK = 64
HV = 128
BLOCK = 64
epsilon = 1e-06
gate_divisor = 16.0
highest_precision = lax.Precision.HIGHEST


def passed_along(value, axis, steps):
    count = lax.axis_size(axis)
    first, last = (max(0, -steps), min(count, count - steps))
    return lax.ppermute(value, axis, [(source, source + steps) for source in range(first, last)])


def entering(array, axis, join, neutral):
    place = lax.axis_index(axis)
    gathered = jax.tree.map(
        lambda a, kind: lax.all_gather(a.astype(kind), axis), array, (jnp.bfloat16, jnp.bfloat16)
    )
    state = jax.tree.map(lambda a, e: jnp.zeros_like(a) + jnp.asarray(e, a.dtype), array, neutral)

    def one(step, state):
        return join(
            state,
            jax.tree.map(
                lambda a, own: lax.dynamic_index_in_dim(a, step, 0, False).astype(own.dtype),
                gathered,
                array,
            ),
        )

    return lax.fori_loop(0, place, one, state)


def project(hidden, weight):
    return jnp.dot(hidden, weight, preferred_element_type=jnp.float32)


def rounded(values_f32):
    return lax.optimization_barrier(values_f32.astype(jnp.bfloat16)).astype(jnp.float32)


def fold_rows(normed, portions):
    return tuple((project(normed, portion) for portion in portions))


def conv_branch(conv_a, conv_gate, conv_weight, conv_gain):
    gated = (rounded(conv_a) * jax.nn.sigmoid(rounded(conv_gate))).astype(jnp.bfloat16)
    rim_rows = conv_weight.shape[0] - 1
    row_count = gated.shape[0]
    earlier = passed_along(gated[row_count - rim_rows :], "sp", 1)
    extended = jnp.concatenate([earlier, gated], axis=0).astype(jnp.float32)
    conv_sum = jnp.zeros(gated.shape, jnp.float32)
    for tap_index in range(conv_weight.shape[0]):
        conv_sum = (
            conv_sum + conv_weight[tap_index][None, :] * extended[tap_index : tap_index + row_count]
        )
    row_sums, row_squares = lax.psum(
        (jnp.sum(conv_sum, axis=1), jnp.sum(conv_sum * conv_sum, axis=1)), "tp"
    )
    mean_val = (row_sums / D_CONV)[:, None]
    square_mean = (row_squares / D_CONV)[:, None]
    conv_norm = (
        (conv_sum - mean_val) * lax.rsqrt(square_mean - mean_val * mean_val + epsilon) * conv_gain
    )
    return jax.nn.silu(conv_norm).astype(jnp.bfloat16)


def chain_step(earlier, later):
    return (earlier[0] * later[0], earlier[1] * later[0][:, :, None] + later[1])


def gla_branch(
    query, keys, values, out_gate, decay_pre, decay_bias, decay_extra, head_gain, init_state
):
    row_count = query.shape[0]
    local_heads = init_state.shape[0]
    blocks = row_count // BLOCK
    log_decay = jax.nn.log_sigmoid(decay_pre + decay_bias) / gate_divisor + decay_extra

    def to_heads(array, width):
        return array.reshape(blocks, BLOCK, local_heads, width).transpose(0, 2, 1, 3)

    query_heads = to_heads(rounded(query), HK) * HK ** (-0.5)
    key_heads = to_heads(rounded(keys), HK)
    value_heads = to_heads(rounded(values), HV)
    cum_log = jnp.cumsum(to_heads(log_decay, HK), axis=2)
    block_total = cum_log[:, :, -1:, :]
    query_decayed = query_heads * jnp.exp(cum_log)
    key_inverse = key_heads * jnp.exp(-cum_log)
    key_to_end = key_heads * jnp.exp(block_total - cum_log)
    causal = jnp.tril(jnp.ones((BLOCK, BLOCK), dtype=bool))
    scores = jnp.where(
        causal,
        jnp.einsum("nhik,nhjk->nhij", query_decayed, key_inverse, precision=highest_precision),
        0.0,
    )
    within = jnp.einsum("nhij,nhjv->nhiv", scores, value_heads, precision=highest_precision)

    def advance(state_current, block_items):
        query_block, key_block, value_block, decay_block = block_items
        carried_state = jnp.einsum(
            "yau,yub->yab", query_block, state_current, precision=highest_precision
        )
        state_following = state_current * decay_block[:, 0, :, None] + jnp.einsum(
            "tie,tis->tes", key_block, value_block, precision=highest_precision
        )
        return (state_following, carried_state)

    zero_state = jnp.zeros(init_state.shape, jnp.float32)
    local_end, carried_out = lax.scan(
        advance, zero_state, (query_decayed, key_to_end, value_heads, jnp.exp(block_total))
    )
    block_sums = block_total[:, :, 0, :]
    device_log = jnp.sum(block_sums, axis=0)
    prefix_log = jnp.cumsum(block_sums, axis=0) - block_sums
    before_decay, before_state = entering(
        (jnp.exp(device_log), local_end),
        "sp",
        chain_step,
        (jnp.ones_like(device_log), jnp.zeros_like(local_end)),
    )
    state_entering = before_state + init_state * before_decay[:, :, None]
    query_since_beginning = query_decayed * jnp.exp(prefix_log)[:, :, None, :]
    incoming_state = jnp.einsum(
        "oltu,luf->oltf", query_since_beginning, state_entering, precision=highest_precision
    )
    attn = within + carried_out + incoming_state
    normal_attn = (
        attn * lax.rsqrt(jnp.mean(attn * attn, axis=-1, keepdims=True) + epsilon) * head_gain
    )
    normal_attn = normal_attn.transpose(0, 2, 1, 3).reshape(row_count, local_heads * HV)
    return (normal_attn * jax.nn.silu(rounded(out_gate))).astype(jnp.bfloat16)


def per_device(
    tokens,
    norm_gain,
    w_conv_a,
    w_conv_gate,
    conv_weight,
    conv_gain,
    w_query,
    w_key,
    w_value,
    w_outgate,
    w_decay,
    decay_bias,
    decay_extra,
    head_gain,
    init_state,
    w_out_conv,
    w_out_gla,
):
    features = lax.all_gather(tokens, "tp", axis=1, tiled=True)
    widened = features.astype(jnp.float32)
    normed = (
        widened
        * lax.rsqrt(jnp.mean(widened * widened, axis=-1, keepdims=True) + epsilon)
        * norm_gain
    ).astype(jnp.bfloat16)
    projected = fold_rows(
        normed,
        (
            lax.all_gather(w_conv_a, "sp", axis=0, tiled=True),
            lax.all_gather(w_conv_gate, "sp", axis=0, tiled=True),
            lax.all_gather(w_query, "sp", axis=0, tiled=True),
            lax.all_gather(w_key, "sp", axis=0, tiled=True),
            lax.all_gather(w_value, "sp", axis=0, tiled=True),
            lax.all_gather(w_outgate, "sp", axis=0, tiled=True),
            lax.all_gather(w_decay, "sp", axis=0, tiled=True),
        ),
    )
    conv_proj = projected[:2]
    conv_out = conv_branch(conv_proj[0], conv_proj[1], conv_weight, conv_gain)
    gla_proj = projected[2:]
    gla_out = gla_branch(
        gla_proj[0],
        gla_proj[1],
        gla_proj[2],
        gla_proj[3],
        gla_proj[4],
        decay_bias,
        decay_extra,
        head_gain,
        init_state,
    )
    out_conv, out_gla = (
        lax.all_gather(w_out_conv, "sp", axis=1, tiled=True),
        lax.all_gather(w_out_gla, "sp", axis=1, tiled=True),
    )
    return lax.psum_scatter(
        (project(conv_out, out_conv) + project(gla_out, out_gla)).astype(jnp.bfloat16),
        "tp",
        scatter_dimension=0,
        tiled=True,
    )


def solution(mesh):
    placed = (
        P("sp", "tp"),
        P(),
        P("sp", "tp"),
        P("sp", "tp"),
        P(None, "tp"),
        P("tp"),
        P("sp", "tp"),
        P("sp", "tp"),
        P("sp", "tp"),
        P("sp", "tp"),
        P("sp", "tp"),
        P("tp"),
        P("sp", "tp"),
        P(),
        P("tp", None, None),
        P("tp", "sp"),
        P("tp", "sp"),
    )
    return jax.shard_map(
        per_device, mesh=mesh, in_specs=placed, out_specs=P(("sp", "tp"), None), check_vma=False
    )
```

profile of v0, /device:TPU:0, one launch (start us, length us, event | category | flops | bytes accessed | tf_op | source)
XLA Modules:
  0.0 656.3 jit_solution(9338845575659341172)
XLA Ops:
  12.8 12.5 %all-gather.15.cloned.1.call-done = bf16[1024,2048]{1,0:T(8,128)(2,1)} async-done(((bf16[1024,1024]{1,0:T(8,128)(2,1)}), bf16[1024,2048]{1,0:T(8,128)(2,1)}) %all-gather.15.cloned.1.call-update) | async-done | bytes 4194320 | tf_op jit(solution)/shard_map/all_gather | solution.py:161
  25.3 3.2 fusion.13
  28.8 3.0 fusion.15
  31.7 52.6 %all-gather.25.cloned.1.call-done = bf16[2048,256]{1,0:T(8,128)(2,1)} async-done(((bf16[128,256]{1,0:T(8,128)(2,1)}), bf16[2048,256]{1,0:T(8,128)(2,1)}) %all-gather.25.cloned.1.call-update) | async-done | bytes 1048592 | tf_op jit(solution)/shard_map/all_gather | solution.py:177
  84.4 4.2 fusion.67
  93.2 47.9 %all-gather.23.cloned.1.call-done = bf16[2048,256]{1,0:T(8,128)(2,1)} async-done(((bf16[128,256]{1,0:T(8,128)(2,1)}), bf16[2048,256]{1,0:T(8,128)(2,1)}) %all-gather.23.cloned.1.call-update) | async-done | bytes 1048592 | tf_op jit(solution)/shard_map/all_gather | solution.py:173
  141.1 3.7 convolution_convert_fusion.5
  147.1 50.5 %all-gather.27.cloned.1.call-done = bf16[2048,256]{1,0:T(8,128)(2,1)} async-done(((bf16[128,256]{1,0:T(8,128)(2,1)}), bf16[2048,256]{1,0:T(8,128)(2,1)}) %all-gather.27.cloned.1.call-update) | async-done | bytes 1048592 | tf_op jit(solution)/shard_map/all_gather | solution.py:174
  197.6 3.7 convolution_convert_fusion.4
  201.4 2.3 reshape.76
  203.7 7.8 %bitcast_multiply_fusion.1 = (f32[16,4,64,64]{3,0,1,2:T(8,128)}, f32[16,4,64,64]{3,0,1,2:T(8,128)}, f32[16,4,64,64]{3,0,1,2:T(8,128)}, f32[16,4,64,64]{3,0,1,2:T(8,128)S(1)}) fusion(f32[16,4,64,64]{3,0,1,2:T(8,128)} %copy-done.1, f32[16,64,4,64]{3,2,1,0:T(4,128)} %reshape.76, f32[16,4,64]{2,0,1:T(8,128)S(1)} %get-tuple-element.156, ...), kind=kLoop, calls=%fused_computation.97 | loop fusion | flops 1572864 | bytes 7372800 | tf_op jit(solution)/shard_map/mul | solution.py:96
  211.5 2.6 copy.36
  214.1 45.4 %all-gather.29.cloned.1.call-done = bf16[2048,512]{1,0:T(8,128)(2,1)} async-done(((bf16[128,512]{1,0:T(8,128)(2,1)}), bf16[2048,512]{1,0:T(8,128)(2,1)}) %all-gather.29.cloned.1.call-update) | async-done | bytes 2097168 | tf_op jit(solution)/shard_map/all_gather | solution.py:175
  259.5 6.2 convolution_convert_fusion.1
  268.6 83.0 %while.26 = (s32[]{:T(128)}, f32[4,64,128]{2,1,0:T(8,128)S(1)}, f32[16,4,64,128]{3,2,1,0:T(8,128)}, f32[16,4,1,64]{3,0,1,2:T(8,128)}, f32[16,4,64,64]{3,0,1,2:T(...) while((s32[]{:T(128)}, f32[4,64,128]{2,1,0:T(8,128)S(1)}, ...), condition=%wide.region_7.8_spmd.clone, body=%wide.region_6.7_spmd.clone.sunk | while | flops 50462720 | bytes 1118832 | solution.py:117
  355.4 8.7 %fusion.54 = f32[16,4,64,64]{3,2,1,0:T(8,128)} fusion(f32[16,4,64,64]{3,0,1,2:T(8,128)} %get-tuple-element.152, f32[16,4,64,64]{3,0,1,2:T(8,128)S(1)} %get-tuple-element.155), kind=kOutput, calls=%fused_computation.101 | convolution fusion | flops 201326592 | bytes 3145728 | tf_op jit(solution)/shard_map/nhik,nhjk->nhij/dot_general | solution.py:101
  364.2 5.5 convolution_convert_fusion.3
  369.6 13.9 %all-gather.19.cloned.1.call-done = bf16[2048,512]{1,0:T(8,128)(2,1)} async-done(((bf16[128,512]{1,0:T(8,128)(2,1)}), bf16[2048,512]{1,0:T(8,128)(2,1)}) %all-gather.19.cloned.1.call-update) | async-done | bytes 2097168 | tf_op jit(solution)/shard_map/all_gather | solution.py:172
  383.5 5.2 convolution_convert_fusion.2
  389.3 3.2 collective-permute-start
  392.5 53.0 %all-gather.31.cloned.1.call-done = bf16[2048,512]{1,0:T(8,128)(2,1)} async-done(((bf16[128,512]{1,0:T(8,128)(2,1)}), bf16[2048,512]{1,0:T(8,128)(2,1)}) %all-gather.31.cloned.1.call-update) | async-done | bytes 2097168 | tf_op jit(solution)/shard_map/all_gather | solution.py:176
  445.5 6.2 convolution_convert_fusion
  451.7 39.0 %all-gather.2 = bf16[16,4,64]{2,1,0:T(4,128)(2,1)S(1)} all-gather(bf16[1,4,64]{2,1,0:T(4,128)(2,1)S(1)} %fusion.85), channel_id=2, replica_groups=mesh['sp'=16,'tp'=2] {'sp'}, dimensions={0}, use_global_device_ids=true | all-gather | bytes 8704 | tf_op jit(solution)/shard_map/all_gather | solution.py:24
  491.0 9.5 %fusion.90 = (f32[1024]{0:T(1024)S(1)}, f32[1024]{0:T(1024)S(1)}, f32[1024,512]{1,0:T(8,128)}) fusion(f32[1054,512]{1,0:T(8,128)S(1)} %maximum_convert_fusion, f32[512]{0:T(512)S(1)} %bitcast.155, f32[512]{0:T(512)S(1)} %bitcast.156, f32[512]{0:T(512)S(1)} %bitcast.127, f32[512]{0:T(512)S(1)} %bitcast.128, f32[512]{0:T(512)S(1)} %bitcast.129, ...), kind=kLoop, calls=%fused_computation.160 | loop fusion | flops 33552384 | bytes 67180544 | tf_op jit(solution)/shard_map/reduce_sum | solution.py:65
  500.5 2.5 all-reduce
  502.9 7.0 %all-gather.21.cloned.1.call-done = bf16[512,2048]{1,0:T(8,128)(2,1)} async-done(((bf16[512,128]{1,0:T(8,128)(2,1)}), bf16[512,2048]{1,0:T(8,128)(2,1)}) %all-gather.21.cloned.1.call-update) | async-done | bytes 2097168 | tf_op jit(solution)/shard_map/all_gather | solution.py:195
  509.9 8.3 %fusion.63 = f32[1024,2048]{1,0:T(8,128)} fusion(bf16[512,2048]{1,0:T(8,128)(2,1)} %all-gather.21.cloned.1.call-done, f32[1024,512]{1,0:T(8,128)} %get-tuple-element.151, f32[512]{0:T(512)S(1)} %copy-done.9, f32[1024]{0:T(1024)S(1)} %get-tuple-element.192, f32[1024]{0:T(1024)S(1)} %get-tuple-element.191), kind=kOutput, calls=%fused_computation.121 | convolution fusion | flops 2151677952 | bytes 12593152 | tf_op jit(solution)/shard_map/dot_general | solution.py:42
  518.2 47.6 %all-gather.35.cloned.1.call-done = bf16[64,64,128]{2,1,0:T(8,128)(2,1)} async-done(((bf16[4,64,128]{2,1,0:T(8,128)(2,1)}), bf16[64,64,128]{2,1,0:T(8,128)(2,1)}) %all-gather.35.cloned.1.call-update) | async-done | bytes 1048592 | tf_op jit(solution)/shard_map/all_gather | solution.py:24
  565.9 3.0 fusion.50
  573.1 57.3 %all-gather.33.cloned.1.call-done = bf16[512,2048]{1,0:T(8,128)(2,1)} async-done(((bf16[512,128]{1,0:T(8,128)(2,1)}), bf16[512,2048]{1,0:T(8,128)(2,1)}) %all-gather.33.cloned.1.call-update) | async-done | bytes 2097168 | tf_op jit(solution)/shard_map/all_gather | solution.py:196
  630.4 8.5 %add_convert_fusion = bf16[1024,2048]{1,0:T(8,128)(2,1)} fusion(f32[1024,2048]{1,0:T(8,128)} %fusion.63, bf16[512,2048]{1,0:T(8,128)(2,1)} %all-gather.33.cloned.1.call-done, bf16[1024,512]{1,0:T(8,128)(2,1)S(1)} %copy-done.11, f32[128,8,4,128]{3,2,1,0:T(4,128)S(1)} %bitcast.123), kind=kOutput, calls=%fused_computation.24 | convolution fusion | flops 2155347968 | bytes 17825792 | tf_op jit(solution)/shard_map/dot_general | solution.py:42
  638.9 10.4 %reduce-scatter.2.cloned.1.call-done = bf16[512,2048]{1,0:T(8,128)(2,1)} async-done(((bf16[1024,2048]{1,0:T(8,128)(2,1)}), bf16[512,2048]{1,0:T(8,128)(2,1)}) %reduce-scatter.2.cloned.1.call-update) | async-done | bytes 2097168 | tf_op jit(solution)/shard_map/reduce_scatter | solution.py:198
  (158 shorter events, 107.4 us)
Async XLA Ops:
  6.5 18.8 %all-gather.15.cloned.1.call-start = ((), (), s32[]{:S(2)}) async-start(), calls=%async_computation.1 | async-start | bytes 6291456 | tf_op jit(solution)/shard_map/all_gather | solution.py:161
  7.3 77.1 %all-gather.25.cloned.1.call-start = ((), (), s32[]{:S(2)}) async-start(), calls=%async_computation.6 | async-start | bytes 1114112 | tf_op jit(solution)/shard_map/all_gather | solution.py:177
  8.0 133.1 %all-gather.23.cloned.1.call-start = ((), (), s32[]{:S(2)}) async-start(), calls=%async_computation.5 | async-start | bytes 1114112 | tf_op jit(solution)/shard_map/all_gather | solution.py:173
  8.7 188.9 %all-gather.27.cloned.1.call-start = ((), (), s32[]{:S(2)}) async-start(), calls=%async_computation.7 | async-start | bytes 1114112 | tf_op jit(solution)/shard_map/all_gather | solution.py:174
  9.3 250.2 %all-gather.29.cloned.1.call-start = ((), (), s32[]{:S(2)}) async-start(), calls=%async_computation.8 | async-start | bytes 2228224 | tf_op jit(solution)/shard_map/all_gather | solution.py:175
  9.9 354.3 %all-gather.17.cloned.1.call-start = ((), (), s32[]{:S(2)}) async-start(), calls=%async_computation.2 | async-start | bytes 2228224 | tf_op jit(solution)/shard_map/all_gather | solution.py:171
  10.5 373.0 %all-gather.19.cloned.1.call-start = ((), (), s32[]{:S(2)}) async-start(), calls=%async_computation.3 | async-start | bytes 2228224 | tf_op jit(solution)/shard_map/all_gather | solution.py:172
  11.2 434.3 %all-gather.31.cloned.1.call-start = ((), (), s32[]{:S(2)}) async-start(), calls=%async_computation.9 | async-start | bytes 2228224 | tf_op jit(solution)/shard_map/all_gather | solution.py:176
  12.0 497.9 %all-gather.21.cloned.1.call-start = ((), (), s32[]{:S(2)}) async-start(), calls=%async_computation.4 | async-start | bytes 2228224 | tf_op jit(solution)/shard_map/all_gather | solution.py:195
  12.7 553.1 %all-gather.35.cloned.1.call-start = ((), (), s32[]{:S(2)}) async-start(), calls=%async_computation.12 | async-start | bytes 1114112 | tf_op jit(solution)/shard_map/all_gather | solution.py:24
  12.8 15.8 %copy-start.6 = (f32[2048]{0:T(1024)S(1)}, f32[2048]{0:T(1024)}, u32[]{:S(2)}) copy-start(f32[2048]{0:T(1024)} %param.22) | copy-start | bytes 24580
  25.3 3.4 copy-start
  28.7 55.6 %copy-start.8 = (f32[1024,256]{1,0:T(8,128)S(1)}, f32[1024,256]{1,0:T(8,128)}, u32[]{:S(2)}) copy-start(f32[1024,256]{1,0:T(8,128)} %param.33) | copy-start | bytes 3145732
  28.7 55.6 %copy-start.10 = (f32[256]{0:T(256)S(1)}, f32[256]{0:T(256)}, u32[]{:S(2)}) copy-start(f32[256]{0:T(256)} %param.32) | copy-start | bytes 3076
  91.2 1.3 copy-start.1
  352.3 278.1 %all-gather.33.cloned.1.call-start = ((), (), s32[]{:S(2)}) async-start(), calls=%async_computation.10 | async-start | bytes 2228224 | tf_op jit(solution)/shard_map/all_gather | solution.py:196
  353.0 296.3 %reduce-scatter.2.cloned.1.call-start = ((), (), s32[]{:S(2)}) async-start(), calls=%async_computation.11 | async-start | bytes 6291456 | tf_op jit(solution)/shard_map/reduce_scatter | solution.py:198
  389.3 101.3 %collective-permute-start = (bf16[30,512]{1,0:T(8,128)(2,1)S(1)}, bf16[30,512]{1,0:T(8,128)(2,1)S(1)}, u32[]{:S(2)}, u32[]{:S(2)}) collective-permute-start(bf16[30,512]{1,0:T(8,128)(2,1)S(1)} %slice.256), channel_id=1, source_target_pairs={{0,2},{2,4},{4,6},{6,8},{8,10},{10,12},{12,14},{14,16},{16,18},{18... | collective-permute-start | bytes 92168 | tf_op jit(solution)/shard_map/ppermute | solution.py:18
  491.0 19.0 %copy-start.9 = (f32[512]{0:T(512)S(1)}, f32[512]{0:T(512)}, u32[]{:S(2)}) copy-start(f32[512]{0:T(512)} %param.26) | copy-start | bytes 6148
  509.9 56.0 %copy-start.2 = (f32[16,4,64,64]{3,0,1,2:T(8,128)S(1)}, f32[16,4,64,64]{3,0,1,2:T(8,128)}, u32[]{:S(2)}) copy-start(f32[16,4,64,64]{3,0,1,2:T(8,128)} %get-tuple-element.154) | copy-start | bytes 3145732
  518.2 47.7 %copy-start.5 = (f32[4,64,128]{2,1,0:T(8,128)S(1)}, f32[4,64,128]{2,1,0:T(8,128)}, u32[]{:S(2)}) copy-start(f32[4,64,128]{2,1,0:T(8,128)} %param.35) | copy-start | bytes 393220
  565.9 3.1 copy-start.3
  565.9 3.1 copy-start.4
  569.0 1.9 copy-start.7
  571.6 58.7 %copy-start.11 = (bf16[1024,512]{1,0:T(8,128)(2,1)S(1)}, bf16[1024,512]{1,0:T(8,128)(2,1)}, u32[]{:S(2)}) copy-start(bf16[1024,512]{1,0:T(8,128)(2,1)} %convolution_convert_fusion) | copy-start | bytes 3145732
Sparse Core Ops, SparseCore 0:
  8.9 16.3 all-gather.14
  28.1 56.2 all-gather.24
  87.1 53.9 all-gather.22
  143.7 53.9 all-gather.26
  200.3 59.2 all-gather.28
  262.1 59.2 all-gather.16
  324.2 59.2 all-gather.18
  386.3 59.1 all-gather.30
  448.2 61.6 all-gather.20
  512.5 53.2 all-gather.34
  568.5 61.7 all-gather.32
  639.0 10.2 reduce-scatter.1
where the time goes:
time: 663 us; the launch traced here: 656 us
  waiting for transfers between devices  405 us (61%)
  matrix products  113 us (17%)
  local copies, waits for them, and re-layouts  49.1 us (7%)
  blocking collectives  41.4 us (6%)
  other arithmetic  29.9 us (5%)
  between operations  14.1 us (2%)
    all_gather x1, waiting for transfers between devices, per_device(): lax.all_gather(w_out_gla, 'sp', axis=1, tiled=True)  57.3 us
    all_gather x1, waiting for transfers between devices, per_device(): lax.all_gather(w_outgate, 'sp', axis=0, tiled=True)  53 us
    all_gather x1, waiting for transfers between devices, per_device(): lax.all_gather(w_decay, 'sp', axis=0, tiled=True)  52.6 us
    dot_general x9, matrix products, project(): return jnp.dot(hidden, weight, preferred_element_type=jnp.float32)  51.5 us
    all_gather x1, waiting for transfers between devices, per_device(): lax.all_gather(w_key, 'sp', axis=0, tiled=True)  50.5 us
    all_gather x1, waiting for transfers between devices, per_device(): lax.all_gather(w_query, 'sp', axis=0, tiled=True)  47.9 us
    all_gather x1, waiting for transfers between devices, entering(): lax.all_gather(a.astype(kind), axis)  47.6 us
    all_gather x1, waiting for transfers between devices, per_device(): lax.all_gather(w_value, 'sp', axis=0, tiled=True)  45.4 us
  transfers between devices with their start and end apart: 13, of which 11 were waited for; matrix products, arithmetic and copies ran while one was open for 28% of the time, Pallas kernels for 0%

commit v1 on v0

--- a/solution.py
+++ b/solution.py
@@ -10,6 +10,12 @@
 epsilon = 1e-06
 gate_divisor = 16.0
 highest_precision = lax.Precision.HIGHEST
+
+
+def all_parts(x, name, d):
+    pieces = lax.all_gather(x, name, axis=0, tiled=False)
+    whole = jnp.concatenate(pieces, axis=d)
+    return whole
 
 
 def passed_along(value, axis, steps):
@@ -193,7 +199,7 @@
     )
     out_conv, out_gla = (
         lax.all_gather(w_out_conv, "sp", axis=1, tiled=True),
-        lax.all_gather(w_out_gla, "sp", axis=1, tiled=True),
+        all_parts(w_out_gla, "sp", 1),
     )
     return lax.psum_scatter(
         (project(conv_out, out_conv) + project(gla_out, out_gla)).astype(jnp.bfloat16),

time: 663 us -> 681 us (1.027)
  waiting for transfers between devices: 405 us -> 421 us
    reduce_scatter x1, waiting for transfers between devices: 10.4 us -> 26.5 us  [per_device(): lax.psum_scatter((project(conv_out, out_conv) + project(gla_out, out_gla)...]
    all_gather x1, waiting for transfers between devices: 13.9 us -> 25.6 us  [per_device(): lax.all_gather(w_conv_gate, 'sp', axis=0, tiled=True)]
    all_gather x1, waiting for transfers between devices: 53 us -> 44.6 us  [per_device(): lax.all_gather(w_outgate, 'sp', axis=0, tiled=True)]
  transfers between devices with their start and end apart: 13 -> 13, of which waited for: 11 -> 11; matrix products, arithmetic and copies ran while one was open for 28% -> 26% of each run, Pallas kernels for 0% -> 0%
where the time goes in v1:
time: 681 us; the launch traced here: 674 us
  waiting for transfers between devices  421 us (62%)
  matrix products  108 us (16%)
  local copies, waits for them, and re-layouts  53.7 us (8%)
  blocking collectives  41.2 us (6%)
  other arithmetic  30.9 us (5%)
  between operations  14.7 us (2%)
    all_gather x1, waiting for transfers between devices, all_parts(): pieces = lax.all_gather(x, name, axis=0, tiled=False)  58.5 us
    all_gather x1, waiting for transfers between devices, per_device(): lax.all_gather(w_decay, 'sp', axis=0, tiled=True)  52.6 us
    all_gather x1, waiting for transfers between devices, per_device(): lax.all_gather(w_key, 'sp', axis=0, tiled=True)  50.5 us
    dot_general x9, matrix products, project(): return jnp.dot(hidden, weight, preferred_element_type=jnp.float32)  48.4 us
    all_gather x1, waiting for transfers between devices, entering(): lax.all_gather(a.astype(kind), axis)  47.7 us
    all_gather x1, waiting for transfers between devices, per_device(): lax.all_gather(w_query, 'sp', axis=0, tiled=True)  47.1 us
    all_gather x1, waiting for transfers between devices, per_device(): lax.all_gather(w_value, 'sp', axis=0, tiled=True)  45.5 us
    all_gather x1, waiting for transfers between devices, per_device(): lax.all_gather(w_outgate, 'sp', axis=0, tiled=True)  44.6 us
  transfers between devices with their start and end apart: 13, of which 11 were waited for; matrix products, arithmetic and copies ran while one was open for 26% of the time, Pallas kernels for 0%

profile of v1, /device:TPU:0, one launch (start us, length us, event | category | flops | bytes accessed | tf_op | source)
XLA Modules:
  0.0 673.7 jit_solution(12933443379926332688)
XLA Ops:
  14.7 58.5 %all-gather.36.cloned.1.call-done = bf16[8192,128]{1,0:T(8,128)(2,1)} async-done(((bf16[512,128]{1,0:T(8,128)(2,1)}), bf16[8192,128]{1,0:T(8,128)(2,1)}) %all-gather.36.cloned.1.call-update) | async-done | bytes 2097168 | tf_op jit(solution)/shard_map/all_gather | solution.py:16
  73.2 3.9 copy.69
  77.2 10.1 %all-gather.16.cloned.1.call-done = bf16[1024,2048]{1,0:T(8,128)(2,1)} async-done(((bf16[1024,1024]{1,0:T(8,128)(2,1)}), bf16[1024,2048]{1,0:T(8,128)(2,1)}) %all-gather.16.cloned.1.call-update) | async-done | bytes 4194320 | tf_op jit(solution)/shard_map/all_gather | solution.py:167
  87.3 3.2 fusion.13
  90.7 3.0 fusion.15
  93.8 52.6 %all-gather.26.cloned.1.call-done = bf16[2048,256]{1,0:T(8,128)(2,1)} async-done(((bf16[128,256]{1,0:T(8,128)(2,1)}), bf16[2048,256]{1,0:T(8,128)(2,1)}) %all-gather.26.cloned.1.call-update) | async-done | bytes 1048592 | tf_op jit(solution)/shard_map/all_gather | solution.py:183
  146.3 4.2 fusion.67
  155.8 47.1 %all-gather.24.cloned.1.call-done = bf16[2048,256]{1,0:T(8,128)(2,1)} async-done(((bf16[128,256]{1,0:T(8,128)(2,1)}), bf16[2048,256]{1,0:T(8,128)(2,1)}) %all-gather.24.cloned.1.call-update) | async-done | bytes 1048592 | tf_op jit(solution)/shard_map/all_gather | solution.py:179
  202.9 3.7 convolution_convert_fusion.5
  209.0 50.5 %all-gather.28.cloned.1.call-done = bf16[2048,256]{1,0:T(8,128)(2,1)} async-done(((bf16[128,256]{1,0:T(8,128)(2,1)}), bf16[2048,256]{1,0:T(8,128)(2,1)}) %all-gather.28.cloned.1.call-update) | async-done | bytes 1048592 | tf_op jit(solution)/shard_map/all_gather | solution.py:180
  259.5 3.7 convolution_convert_fusion.4
  265.4 7.8 %bitcast_multiply_fusion.1 = (f32[16,4,64,64]{3,0,1,2:T(8,128)}, f32[16,4,64,64]{3,0,1,2:T(8,128)}, f32[16,4,64,64]{3,0,1,2:T(8,128)}, f32[16,4,64,64]{3,0,1,2:T(8,128)S(1)}) fusion(f32[16,4,64,64]{3,0,1,2:T(8,128)} %copy-done.1, f32[16,64,4,64]{3,2,1,0:T(4,128)} %reshape.84, f32[16,4,64]{2,0,1:T(8,128)S(1)} %get-tuple-element.170, ...), kind=kLoop, calls=%fused_computation.95 | loop fusion | flops 1572864 | bytes 7372800 | tf_op jit(solution)/shard_map/mul | solution.py:102
  273.2 2.6 copy.59
  275.8 45.5 %all-gather.30.cloned.1.call-done = bf16[2048,512]{1,0:T(8,128)(2,1)} async-done(((bf16[128,512]{1,0:T(8,128)(2,1)}), bf16[2048,512]{1,0:T(8,128)(2,1)}) %all-gather.30.cloned.1.call-update) | async-done | bytes 2097168 | tf_op jit(solution)/shard_map/all_gather | solution.py:181
  321.3 6.1 convolution_convert_fusion.1
  330.4 83.1 %while.26 = (s32[]{:T(128)}, f32[4,64,128]{2,1,0:T(8,128)S(1)}, f32[16,4,64,128]{3,2,1,0:T(8,128)}, f32[16,4,1,64]{3,0,1,2:T(8,128)}, f32[16,4,64,64]{3,0,1,2:T(...) while((s32[]{:T(128)}, f32[4,64,128]{2,1,0:T(8,128)S(1)}, ...), condition=%wide.region_7.8_spmd.clone, body=%wide.region_6.7_spmd.clone.sunk | while | flops 50462720 | bytes 1118832 | solution.py:123
  413.5 6.2 convolution_convert_fusion.3
  419.8 25.6 %all-gather.20.cloned.1.call-done = bf16[2048,512]{1,0:T(8,128)(2,1)} async-done(((bf16[128,512]{1,0:T(8,128)(2,1)}), bf16[2048,512]{1,0:T(8,128)(2,1)}) %all-gather.20.cloned.1.call-update) | async-done | bytes 2097168 | tf_op jit(solution)/shard_map/all_gather | solution.py:178
  445.4 5.3 convolution_convert_fusion.2
  452.2 3.2 collective-permute-start
  455.4 7.3 %fusion.54 = f32[16,4,64,64]{3,2,1,0:T(8,128)} fusion(f32[16,4,64,64]{3,0,1,2:T(8,128)S(1)} %copy-done.2, f32[16,4,64,64]{3,0,1,2:T(8,128)S(1)} %get-tuple-element.169), kind=kOutput, calls=%fused_computation.101 | convolution fusion | flops 201326592 | bytes 3145728 | tf_op jit(solution)/shard_map/nhik,nhjk->nhij/dot_general | solution.py:107
  462.8 44.6 %all-gather.32.cloned.1.call-done = bf16[2048,512]{1,0:T(8,128)(2,1)} async-done(((bf16[128,512]{1,0:T(8,128)(2,1)}), bf16[2048,512]{1,0:T(8,128)(2,1)}) %all-gather.32.cloned.1.call-update) | async-done | bytes 2097168 | tf_op jit(solution)/shard_map/all_gather | solution.py:182
  507.4 6.2 convolution_convert_fusion
  514.6 38.8 %all-gather.3 = bf16[16,4,64]{2,1,0:T(4,128)(2,1)S(1)} all-gather(bf16[1,4,64]{2,1,0:T(4,128)(2,1)S(1)} %fusion.85), channel_id=2, replica_groups=mesh['sp'=16,'tp'=2] {'sp'}, dimensions={0}, use_global_device_ids=true | all-gather | bytes 8704 | tf_op jit(solution)/shard_map/all_gather | solution.py:30
  554.0 9.7 %fusion.90 = (f32[1024]{0:T(1024)S(1)}, f32[1024]{0:T(1024)S(1)}, f32[1024,512]{1,0:T(8,128)}) fusion(f32[1054,512]{1,0:T(8,128)S(1)} %maximum_convert_fusion, f32[512]{0:T(512)S(1)} %bitcast.161, f32[512]{0:T(512)S(1)} %bitcast.162, f32[512]{0:T(512)S(1)} %bitcast.133, f32[512]{0:T(512)S(1)} %bitcast.134, f32[512]{0:T(512)S(1)} %bitcast.135, ...), kind=kLoop, calls=%fused_computation.160 | loop fusion | flops 33552384 | bytes 67180544 | tf_op jit(solution)/shard_map/reduce_sum | solution.py:71
  563.7 2.5 all-reduce
  566.1 5.5 all-gather.22.cloned.1.call-done
  571.6 8.3 %fusion.63 = f32[1024,2048]{1,0:T(8,128)} fusion(bf16[512,2048]{1,0:T(8,128)(2,1)} %all-gather.22.cloned.1.call-done, f32[1024,512]{1,0:T(8,128)} %get-tuple-element.165, f32[512]{0:T(512)S(1)} %copy-done.45, f32[1024]{0:T(1024)S(1)} %get-tuple-element.206, f32[1024]{0:T(1024)S(1)} %get-tuple-element.205), kind=kOutput, calls=%fused_computation.121 | convolution fusion | flops 2151677952 | bytes 12593152 | tf_op jit(solution)/shard_map/dot_general | solution.py:48
  579.9 47.7 %all-gather.34.cloned.1.call-done = bf16[64,64,128]{2,1,0:T(8,128)(2,1)} async-done(((bf16[4,64,128]{2,1,0:T(8,128)(2,1)}), bf16[64,64,128]{2,1,0:T(8,128)(2,1)}) %all-gather.34.cloned.1.call-update) | async-done | bytes 1048592 | tf_op jit(solution)/shard_map/all_gather | solution.py:30
  627.8 3.0 fusion.52
  635.6 4.5 add_convert_fusion
  640.1 26.5 %reduce-scatter.2.cloned.1.call-done = bf16[512,2048]{1,0:T(8,128)(2,1)} async-done(((bf16[1024,2048]{1,0:T(8,128)(2,1)}), bf16[512,2048]{1,0:T(8,128)(2,1)}) %reduce-scatter.2.cloned.1.call-update) | async-done | bytes 2097168 | tf_op jit(solution)/shard_map/reduce_scatter | solution.py:204
  (236 shorter events, 110.7 us)
Async XLA Ops:
  6.5 66.7 %all-gather.36.cloned.1.call-start = ((), (), s32[]{:S(2)}) async-start(), calls=%async_computation.12 | async-start | bytes 2228224 | tf_op jit(solution)/shard_map/all_gather | solution.py:16
  7.3 80.0 %all-gather.16.cloned.1.call-start = ((), (), s32[]{:S(2)}) async-start(), calls=%async_computation.1 | async-start | bytes 6291456 | tf_op jit(solution)/shard_map/all_gather | solution.py:167
  8.0 138.3 %all-gather.26.cloned.1.call-start = ((), (), s32[]{:S(2)}) async-start(), calls=%async_computation.6 | async-start | bytes 1114112 | tf_op jit(solution)/shard_map/all_gather | solution.py:183
  8.7 194.2 %all-gather.24.cloned.1.call-start = ((), (), s32[]{:S(2)}) async-start(), calls=%async_computation.5 | async-start | bytes 1114112 | tf_op jit(solution)/shard_map/all_gather | solution.py:179
  9.3 250.1 %all-gather.28.cloned.1.call-start = ((), (), s32[]{:S(2)}) async-start(), calls=%async_computation.7 | async-start | bytes 1114112 | tf_op jit(solution)/shard_map/all_gather | solution.py:180
  9.9 311.4 %all-gather.30.cloned.1.call-start = ((), (), s32[]{:S(2)}) async-start(), calls=%async_computation.8 | async-start | bytes 2228224 | tf_op jit(solution)/shard_map/all_gather | solution.py:181
  10.5 403.1 %all-gather.18.cloned.1.call-start = ((), (), s32[]{:S(2)}) async-start(), calls=%async_computation.2 | async-start | bytes 2228224 | tf_op jit(solution)/shard_map/all_gather | solution.py:177
  11.2 434.1 %all-gather.20.cloned.1.call-start = ((), (), s32[]{:S(2)}) async-start(), calls=%async_computation.3 | async-start | bytes 2228224 | tf_op jit(solution)/shard_map/all_gather | solution.py:178
  12.0 495.4 %all-gather.32.cloned.1.call-start = ((), (), s32[]{:S(2)}) async-start(), calls=%async_computation.9 | async-start | bytes 2228224 | tf_op jit(solution)/shard_map/all_gather | solution.py:182
  12.7 558.9 %all-gather.22.cloned.1.call-start = ((), (), s32[]{:S(2)}) async-start(), calls=%async_computation.4 | async-start | bytes 2228224 | tf_op jit(solution)/shard_map/all_gather | solution.py:201
  13.3 614.4 %all-gather.34.cloned.1.call-start = ((), (), s32[]{:S(2)}) async-start(), calls=%async_computation.11 | async-start | bytes 1114112 | tf_op jit(solution)/shard_map/all_gather | solution.py:30
  90.7 55.6 %copy-start.44 = (f32[1024,256]{1,0:T(8,128)S(1)}, f32[1024,256]{1,0:T(8,128)}, u32[]{:S(2)}) copy-start(f32[1024,256]{1,0:T(8,128)} %param.33) | copy-start | bytes 3145732
  90.7 55.6 %copy-start.46 = (f32[256]{0:T(256)S(1)}, f32[256]{0:T(256)}, u32[]{:S(2)}) copy-start(f32[256]{0:T(256)} %param.32) | copy-start | bytes 3076
  452.2 101.1 %collective-permute-start = (bf16[30,512]{1,0:T(8,128)(2,1)S(1)}, bf16[30,512]{1,0:T(8,128)(2,1)S(1)}, u32[]{:S(2)}, u32[]{:S(2)}) collective-permute-start(bf16[30,512]{1,0:T(8,128)(2,1)S(1)} %slice.256), channel_id=1, source_target_pairs={{0,2},{2,4},{4,6},{6,8},{8,10},{10,12},{12,14},{14,16},{16,18},{18... | collective-permute-start | bytes 92168 | tf_op jit(solution)/shard_map/ppermute | solution.py:24
  462.8 51.1 %copy-start.42 = (f32[4,64]{1,0:T(4,128)S(1)}, f32[4,64]{1,0:T(4,128)}, u32[]{:S(2)}) copy-start(f32[4,64]{1,0:T(4,128)} %get-tuple-element.172) | copy-start | bytes 3076
  462.8 90.6 %copy-start.6 = (bf16[1024,512]{1,0:T(8,128)(2,1)S(1)}, bf16[1024,512]{1,0:T(8,128)(2,1)}, u32[]{:S(2)}) copy-start(bf16[1024,512]{1,0:T(8,128)(2,1)} %copy-done.5) | copy-start | bytes 3145732
  513.6 40.1 %copy-start.17 = (f32[1,512]{1,0:T(1,128)S(1)}, f32[1,512]{1,0:T(1,128)}, u32[]{:S(2)}) copy-start(f32[1,512]{1,0:T(1,128)} %get-tuple-element.180) | copy-start | bytes 6148
  513.6 40.1 %copy-start.18 = (f32[1,512]{1,0:T(1,128)S(1)}, f32[1,512]{1,0:T(1,128)}, u32[]{:S(2)}) copy-start(f32[1,512]{1,0:T(1,128)} %get-tuple-element.181) | copy-start | bytes 6148
  513.6 40.1 %copy-start.19 = (f32[1,512]{1,0:T(1,128)S(1)}, f32[1,512]{1,0:T(1,128)}, u32[]{:S(2)}) copy-start(f32[1,512]{1,0:T(1,128)} %get-tuple-element.182) | copy-start | bytes 6148
  513.6 40.1 %copy-start.20 = (f32[1,512]{1,0:T(1,128)S(1)}, f32[1,512]{1,0:T(1,128)}, u32[]{:S(2)}) copy-start(f32[1,512]{1,0:T(1,128)} %get-tuple-element.183) | copy-start | bytes 6148
  513.6 40.1 %copy-start.21 = (f32[1,512]{1,0:T(1,128)S(1)}, f32[1,512]{1,0:T(1,128)}, u32[]{:S(2)}) copy-start(f32[1,512]{1,0:T(1,128)} %get-tuple-element.184) | copy-start | bytes 6148
  513.6 40.1 %copy-start.22 = (f32[1,512]{1,0:T(1,128)S(1)}, f32[1,512]{1,0:T(1,128)}, u32[]{:S(2)}) copy-start(f32[1,512]{1,0:T(1,128)} %get-tuple-element.185) | copy-start | bytes 6148
  513.7 40.1 %copy-start.23 = (f32[1,512]{1,0:T(1,128)S(1)}, f32[1,512]{1,0:T(1,128)}, u32[]{:S(2)}) copy-start(f32[1,512]{1,0:T(1,128)} %get-tuple-element.186) | copy-start | bytes 6148
  513.7 40.1 %copy-start.24 = (f32[1,512]{1,0:T(1,128)S(1)}, f32[1,512]{1,0:T(1,128)}, u32[]{:S(2)}) copy-start(f32[1,512]{1,0:T(1,128)} %get-tuple-element.187) | copy-start | bytes 6148
  513.7 40.1 %copy-start.25 = (f32[1,512]{1,0:T(1,128)S(1)}, f32[1,512]{1,0:T(1,128)}, u32[]{:S(2)}) copy-start(f32[1,512]{1,0:T(1,128)} %get-tuple-element.188) | copy-start | bytes 6148
  513.7 40.1 %copy-start.26 = (f32[1,512]{1,0:T(1,128)S(1)}, f32[1,512]{1,0:T(1,128)}, u32[]{:S(2)}) copy-start(f32[1,512]{1,0:T(1,128)} %get-tuple-element.189) | copy-start | bytes 6148
  513.7 40.1 %copy-start.27 = (f32[1,512]{1,0:T(1,128)S(1)}, f32[1,512]{1,0:T(1,128)}, u32[]{:S(2)}) copy-start(f32[1,512]{1,0:T(1,128)} %get-tuple-element.190) | copy-start | bytes 6148
  513.7 40.1 %copy-start.28 = (f32[1,512]{1,0:T(1,128)S(1)}, f32[1,512]{1,0:T(1,128)}, u32[]{:S(2)}) copy-start(f32[1,512]{1,0:T(1,128)} %get-tuple-element.191) | copy-start | bytes 6148
  513.7 40.1 %copy-start.29 = (f32[1,512]{1,0:T(1,128)S(1)}, f32[1,512]{1,0:T(1,128)}, u32[]{:S(2)}) copy-start(f32[1,512]{1,0:T(1,128)} %get-tuple-element.192) | copy-start | bytes 6148
  514.5 152.1 %reduce-scatter.2.cloned.1.call-start = ((), (), s32[]{:S(2)}) async-start(), calls=%async_computation.10 | async-start | bytes 6291456 | tf_op jit(solution)/shard_map/reduce_scatter | solution.py:204
  571.6 56.1 %copy-start.3 = (f32[16,4,64,64]{3,0,1,2:T(8,128)S(1)}, f32[16,4,64,64]{3,0,1,2:T(8,128)}, u32[]{:S(2)}) copy-start(f32[16,4,64,64]{3,0,1,2:T(8,128)} %get-tuple-element.168) | copy-start | bytes 3145732
  579.9 47.8 %copy-start.10 = (f32[4,64,128]{2,1,0:T(8,128)S(1)}, f32[4,64,128]{2,1,0:T(8,128)}, u32[]{:S(2)}) copy-start(f32[4,64,128]{2,1,0:T(8,128)} %param.35) | copy-start | bytes 393220
  (31 other events, 719.1 us)
Sparse Core Ops, SparseCore 0:
  10.1 63.0 all-gather.35
  74.8 12.4 all-gather.15
  90.0 56.2 all-gather.25
  148.9 53.9 all-gather.23
  205.5 53.9 all-gather.27
  262.1 59.2 all-gather.29
  324.1 59.1 all-gather.17
  386.1 59.2 all-gather.19
  448.1 59.1 all-gather.31
  509.9 61.6 all-gather.21
  574.4 53.2 all-gather.33
  640.2 26.3 reduce-scatter.1
